TPU v7x, 32 devices: a whole 2x2x4 slice. The times are simulated.
32 devices in a mesh: fs: 16 (over z, y, x), tp: 2 (over core).
Axes of the slice: x: 2, y: 2, z: 4, core: 2. Of those that a mesh axis runs over, the one named last changes fastest.
Arguments:
- fwd_input: bfloat16 [2048, 2048], P('fs'), may hold values from -6 to 6
- saved_input: bfloat16 [2048, 2048], P('fs'), may hold values from -6 to 6
- out_cotangent: bfloat16 [2048, 2048], P('fs'), may hold values from -6 to 6
- up_weight: bfloat16 [2048, 4096], P('fs', 'tp'), may hold values from -0.125 to 0.125
- down_weight: bfloat16 [4096, 2048], P('tp', 'fs'), may hold values from -0.09375 to 0.09375
- up_grad_sum: float32 [2048, 4096], P('fs', 'tp'), may hold values from -6 to 6
Outputs:
- layer_out: bfloat16 [2048, 2048], P('fs')
- input_grad: bfloat16 [2048, 2048], P('fs')
- up_grad_out: float32 [2048, 4096], P('fs', 'tp')
All inputs are finite; a program needn't handle non-finite values.
Results may differ from a plain program's by a relative error of at most 0.013.
Values may be sent and summed in bfloat16 or wider, within the bound.
A program may use at most 128 MiB of HBM per device.

v0:
```python
import jax
import jax.numpy as jnp
from jax import lax
from jax.sharding import PartitionSpec as P


def per_device(fwd_input, saved_input, out_cotangent, up_weight, down_weight, up_grad_sum):
    row_count = fwd_input.shape[0]
    stacked = jnp.concatenate([fwd_input, saved_input], axis=0)
    up_whole = lax.all_gather(up_weight, "fs", axis=0, tiled=True)
    down_whole = lax.all_gather(down_weight, "fs", axis=1, tiled=True)
    pre_both = jnp.dot(stacked, up_whole, preferred_element_type=jnp.float32)
    pre_fwd = pre_both[:row_count]
    pre_bwd = pre_both[row_count:]
    positive = jnp.maximum(pre_fwd, 0.0)
    hidden = (positive * positive).astype(jnp.bfloat16)
    out_part = jnp.dot(hidden, down_whole, preferred_element_type=jnp.float32)
    layer_out = lax.psum(out_part.astype(jnp.bfloat16), "tp")
    d_hidden = lax.dot_general(
        out_cotangent, down_whole, (((1,), (1,)), ((), ())), preferred_element_type=jnp.float32
    )
    d_pre = (d_hidden * 2.0 * jnp.maximum(pre_bwd, 0.0)).astype(jnp.bfloat16)
    in_part = lax.dot_general(
        d_pre, up_whole, (((1,), (1,)), ((), ())), preferred_element_type=jnp.float32
    )
    input_grad = lax.psum(in_part.astype(jnp.bfloat16), "tp")
    grad_part = lax.psum_scatter(
        lax.dot_general(
            saved_input, d_pre, (((0,), (0,)), ((), ())), preferred_element_type=jnp.float32
        ),
        "fs",
        scatter_dimension=0,
        tiled=True,
    )
    grad_scale = float(row_count * lax.axis_size("fs")) ** (-0.5)
    return (layer_out, input_grad, up_grad_sum + grad_part * grad_scale)


def solution(mesh):
    placed = (
        P("fs", None),
        P("fs", None),
        P("fs", None),
        P("fs", "tp"),
        P("tp", "fs"),
        P("fs", "tp"),
    )
    return jax.shard_map(
        per_device,
        mesh=mesh,
        in_specs=placed,
        out_specs=(P("fs", None), P("fs", None), P("fs", "tp")),
        check_vma=False,
    )
```

profile of v0, /device:TPU:10, one launch (start us, length us, event | category | flops | bytes accessed | tf_op | source)
XLA Modules:
  0.0 664.8 jit_solution(1798604370416390500)
XLA Ops:
  7.2 0.0 copy-start
  7.2 0.0 all-gather.3.cloned.1.call-start
  7.2 0.7 all-gather.3.cloned.1.call-update
  7.9 0.0 all-gather.5.cloned.1.call-start
  8.0 0.7 all-gather.5.cloned.1.call-update
  8.7 0.0 reduce-scatter.2.cloned.1.call-start
  8.7 114.4 %all-gather.3.cloned.1.call-done = bf16[2048,2048]{1,0:T(8,128)(2,1)} async-done(((bf16[128,2048]{1,0:T(8,128)(2,1)}), bf16[2048,2048]{1,0:T(8,128)(2,1)}) %all-gather.3.cloned.1.call-update) | async-done | bytes 8388624 | tf_op jit(solution)/shard_map/all_gather | solution.py:10
  123.1 6.0 fusion.4
  129.2 135.0 %all-gather.5.cloned.1.call-done = bf16[2048,2048]{1,0:T(8,128)(2,1)} async-done(((bf16[2048,128]{1,0:T(8,128)(2,1)}), bf16[2048,2048]{1,0:T(8,128)(2,1)}) %all-gather.5.cloned.1.call-update) | async-done | bytes 8388624 | tf_op jit(solution)/shard_map/all_gather | solution.py:11
  264.2 0.0 copy-done
  264.2 0.0 copy-start.1
  264.2 6.3 fusion.1
  270.5 0.0 copy-done.1
  270.5 8.1 %convolution_bitcast_fusion = f32[2048,2048]{0,1:T(8,128)} fusion(bf16[128,2048]{1,0:T(8,128)(2,1)S(1)} %fusion.1, bf16[128,2048]{1,0:T(8,128)(2,1)S(1)} %copy-done.1), kind=kOutput, calls=%fused_computation | convolution fusion | flops 1073741824 | bytes 17825792 | tf_op jit(solution)/shard_map/dot_general | solution.py:28
  278.7 0.0 reduce-scatter.2.cloned.1.call-update
  278.7 0.0 all-reduce.3.cloned.1.call-start
  278.7 7.1 %convolution_convert_fusion = bf16[128,2048]{1,0:T(8,128)(2,1)} fusion(bf16[128,2048]{1,0:T(8,128)(2,1)S(1)} %fusion.1, bf16[2048,2048]{1,0:T(8,128)(2,1)} %all-gather.3.cloned.1.call-done), kind=kOutput, calls=%fused_computation.3 | convolution fusion | flops 1074003968 | bytes 9437184 | tf_op jit(solution)/shard_map/dot_general | solution.py:23
  285.8 5.9 convolution_convert_fusion.1
  291.7 0.0 all-reduce.3.cloned.1.call-update
  291.7 1.6 copy.9
  293.3 338.6 %reduce-scatter.2.cloned.1.call-done = f32[128,2048]{0,1:T(8,128)} async-done(((f32[2048,2048]{0,1:T(8,128)}), f32[128,2048]{0,1:T(8,128)}) %reduce-scatter.2.cloned.1.call-update) | async-done | bytes 1048592 | tf_op jit(solution)/shard_map/reduce_scatter | solution.py:27
  631.9 1.3 multiply_add_fusion
  633.2 1.3 copy.10
  634.5 19.9 %all-reduce.3.cloned.1.call-done = (bf16[128,2048]{1,0:T(8,128)(2,1)}, bf16[128,2048]{1,0:T(8,128)(2,1)}) async-done(((bf16[128,2048]{1,0:T(8,128)(2,1)}, bf16[128,2048]{1,0:T(8,128)(2,1)}), (bf16[128,2048]{1,0:T(8,128)(2,1)}, bf16[128,2048]{1,0:T(8,128)(2,1)})) %all-reduce.3.cloned.1.call-update) | async-done | bytes 1048592 | tf_op jit(solution)/shard_map/psum | solution.py:18
  654.5 1.9 copy.13
  656.4 1.9 copy.14
Async XLA Ops:
  7.2 257.0 %copy-start = (bf16[128,2048]{1,0:T(8,128)(2,1)S(1)}, bf16[128,2048]{1,0:T(8,128)(2,1)}, u32[]{:S(2)}) copy-start(bf16[128,2048]{1,0:T(8,128)(2,1)} %param.8) | copy-start | bytes 1572868
  7.2 115.9 %all-gather.3.cloned.1.call-start = ((), (), s32[]{:S(2)}) async-start(), calls=%async_computation.1 | async-start | bytes 8912896 | tf_op jit(solution)/shard_map/all_gather | solution.py:10
  7.9 256.3 %all-gather.5.cloned.1.call-start = ((), (), s32[]{:S(2)}) async-start(), calls=%async_computation.2 | async-start | bytes 8912896 | tf_op jit(solution)/shard_map/all_gather | solution.py:11
  8.7 623.2 %reduce-scatter.2.cloned.1.call-start = ((), (), s32[]{:S(2)}) async-start(), calls=%async_computation.3 | async-start | bytes 17825792 | tf_op jit(solution)/shard_map/reduce_scatter | solution.py:27
  264.2 6.3 copy-start.1
  278.7 375.8 %all-reduce.3.cloned.1.call-start = ((), (), s32[]{:S(2)}) async-start(), calls=%async_computation.4 | async-start | bytes 2097152 | tf_op jit(solution)/shard_map/psum | solution.py:18
Sparse Core Ops, SparseCore 0:
  10.8 112.3 all-gather.2
  125.8 138.3 all-gather.4
  278.8 353.0 reduce-scatter.1
  634.7 19.7 all-reduce.2
where the time goes:
time: 666 us; the launch traced here: 665 us
  waiting for transfers between devices  609 us (91%)
  matrix products  33.4 us (5%)
  between operations  13.8 us (2%)
    reduce_scatter x1, waiting for transfers between devices, per_device(): lax.psum_scatter(lax.dot_general(saved_input, d_pre, (((0,), (0,)), ((),...  339 us
    all_gather x1, waiting for transfers between devices, per_device(): down_whole = lax.all_gather(down_weight, 'fs', axis=1, tiled=True)  135 us
    all_gather x1, waiting for transfers between devices, per_device(): up_whole = lax.all_gather(up_weight, 'fs', axis=0, tiled=True)  114 us
    psum x1, waiting for transfers between devices, per_device(): layer_out = lax.psum(out_part.astype(jnp.bfloat16), 'tp')  19.9 us
  transfers between devices with their start and end apart: 4, of which 4 were waited for; matrix products, arithmetic and copies ran while one was open for 3% of the time, Pallas kernels for 0%

commit v1 on v0

v1 whole, which is shorter than its diff:
```python
import functools

import jax
import jax.numpy as jnp
from jax import lax
from jax.experimental import pallas as pl
from jax.experimental.pallas import tpu as pltpu
from jax.sharding import PartitionSpec as P

MESH = pl.DeviceIdType.MESH
F32 = jnp.float32
BF16 = jnp.bfloat16


def remote(src, dst, send_sem, recv_sem, fs, tp):
    return pltpu.make_async_remote_copy(
        src_ref=src,
        dst_ref=dst,
        send_sem=send_sem,
        recv_sem=recv_sem,
        device_id=(fs, tp),
        device_id_type=MESH,
    )


def kernel(
    n, T, B, fwd, saved, cot, up, down_t, out, ing, gout,
    X, W, H, O, tp_in, S, pl_in, G, from_left, from_right,
    lsem, wS, wR, zS, zR, aS, aR, bS, bR, tS, tR, pS, pR, fS, fR, gS, gL, gR, hS, hR,
):
    A = n // B
    f, t = lax.axis_index("fs"), lax.axis_index("tp")
    z, p = lax.div(f, B), lax.rem(f, B)
    rows, D = fwd.shape
    C = rows // T
    Rw, F = up.shape
    Fs = F // B
    tokens = B * rows
    peers = [lax.rem(p + i, B) for i in range(1, B)]
    mates = [lax.rem(t + i, T) for i in range(1, T)]
    has_left, has_right = z > 0, z < A - 1

    def chunk(index):
        return pl.ds(pl.multiple_of(index * C, C), C)

    def cols(index):
        return pl.ds(pl.multiple_of(index * Fs, Fs), Fs)

    barrier = pltpu.get_barrier_semaphore()
    for q in peers:
        pl.semaphore_signal(barrier, inc=1, device_id=(z * B + q, t), device_id_type=MESH)
    for m in mates:
        pl.semaphore_signal(barrier, inc=1, device_id=(f, m), device_id_type=MESH)

    @pl.when(has_left)
    def _():
        pl.semaphore_signal(barrier, inc=1, device_id=(f - B, t), device_id_type=MESH)

    @pl.when(has_right)
    def _():
        pl.semaphore_signal(barrier, inc=1, device_id=(f + B, t), device_id_type=MESH)

    ends = lax.div(z + A - 1, A) + lax.div(A - 1 - z + A - 1, A)
    pl.semaphore_wait(barrier, B - 1 + T - 1 + ends)

    weights = (up, down_t)

    def slice_out(pc, i, q):
        return remote(
            weights[pc].at[:, cols(q)], W.at[pc, f], wS.at[pc, i], wR.at[pc, p], z * B + q, t
        )

    def slice_in(pc, q):
        return remote(
            W.at[pc, z * B + q], W.at[pc, z * B + q], wS.at[pc, 0], wR.at[pc, q], z * B + q, t
        )

    def line(pc, k, q, way, src=None):
        at = k * B + q
        block = W.at[pc, at]
        target = f + B if way == 0 else f - B
        return remote(block if src is None else src, block, zS.at[way, pc, at], zR.at[pc, at], target, t)

    own_w = [
        pltpu.make_async_copy(weights[pc].at[:, cols(p)], W.at[pc, f], lsem.at[pc]) for pc in range(2)
    ]
    for pc in range(2):
        own_w[pc].start()
        for i, q in enumerate(peers):
            slice_out(pc, i, q).start()
        src = weights[pc].at[:, cols(p)]

        @pl.when(has_right)
        def _(pc=pc, src=src):
            line(pc, z, p, 0, src).start()

        @pl.when(has_left)
        def _(pc=pc, src=src):
            line(pc, z, p, 1, src).start()

    acts = (fwd, saved, cot)

    def act_out(j, i, q):
        return remote(acts[j].at[chunk(t)], X.at[j, p, chunk(t)], aS.at[j, i], aR.at[j, p], z * B + q, t)

    def act_in(j, q):
        there = X.at[j, q, chunk(t)]
        return remote(there, there, aS.at[j, 0], aR.at[j, q], z * B + q, t)

    own_x = [pltpu.make_async_copy(acts[j], X.at[j, p], lsem.at[2 + j]) for j in range(3)]
    for j in (1, 2, 0):
        own_x[j].start()
        for i, q in enumerate(peers):
            act_out(j, i, q).start()

    def act_share(i, q, o, m):
        there = X.at[:, q, chunk(t)]
        return remote(there, there, bS.at[i, o], bR.at[q, t], f, m)

    def act_shared(i, q, o, m):
        there = X.at[:, q, chunk(m)]
        return remote(there, there, bS.at[i, o], bR.at[q, m], f, m)

    for pc in range(2):
        for q in peers:
            slice_in(pc, q).wait_recv()

            @pl.when(has_right)
            def _(pc=pc, q=q):
                line(pc, z, q, 0).start()

            @pl.when(has_left)
            def _(pc=pc, q=q):
                line(pc, z, q, 1).start()

    order = [p] + peers
    for s in range(1, A):
        for pc in range(2):
            for q in order:

                @pl.when(z >= s)
                def _(pc=pc, q=q, s=s):
                    line(pc, z - s, q, 0).wait_recv()

                    @pl.when(has_right)
                    def _():
                        line(pc, z - s, q, 0).start()

                @pl.when(z + s < A)
                def _(pc=pc, q=q, s=s):
                    line(pc, z + s, q, 1).wait_recv()

                    @pl.when(has_left)
                    def _():
                        line(pc, z + s, q, 1).start()

        if s == max(A - 2, 1):
            for i, q in enumerate(peers):
                for j in range(3):
                    act_in(j, q).wait_recv()
                for o, m in enumerate(mates):
                    act_share(i, q, o, m).start()

    for copy in own_w + own_x:
        copy.wait()
    for i, q in enumerate(peers):
        for o, m in enumerate(mates):
            act_shared(i, q, o, m).wait_recv()

    wide = min(256, Fs)

    def product(j, pc, at):
        return jnp.dot(
            X[j].reshape(tokens, D), W[pc, :, :, at].reshape(D, wide), preferred_element_type=F32
        )

    @pl.loop(0, Fs // wide)
    def _(c):
        at = pl.ds(pl.multiple_of(c * wide, wide), wide)
        pre = product(1, 0, at)
        d_hidden = product(2, 1, at)
        H[1, :, at] = (d_hidden * 2.0 * jnp.maximum(pre, 0.0)).astype(BF16)

    def to_right(d):
        return remote(G.at[d], from_left.at[d], gS.at[d], gL.at[d], f + B, t)

    def to_left(d):
        return remote(G.at[d], from_right.at[d], gS.at[d], gR.at[d], f - B, t)

    planes = []
    for i in range((A + 1) // 2):
        planes += [A - 1 - i] if A - 1 - i == i else [A - 1 - i, i]
    deep = B * Rw
    for d in planes:
        term = lax.dot_general(
            X[1, :, :, d * deep:(d + 1) * deep].reshape(tokens, deep),
            H[1],
            (((0,), (0,)), ((), ())),
            preferred_element_type=F32,
        )
        G[d] = term.astype(BF16).reshape(B, Rw, Fs)
        if d > 0:

            @pl.when(z == 0)
            def _(d=d):
                to_right(d).start()

        if d < A - 1:

            @pl.when(z == A - 1)
            def _(d=d):
                to_left(d).start()

    pack = max(1, 256 // Rw)

    def spread(o, pc):
        @pl.loop(0, n // pack)
        def _(c):
            block = W[pc, pl.ds(c * pack, pack)].reshape(pack * Rw, Fs)
            part = lax.dot_general(H[o], block, (((1,), (1,)), ((), ())), preferred_element_type=F32)
            at = pl.ds(pl.multiple_of(c * (pack * Rw), pack * Rw), pack * Rw)
            O[o, :, :, at] = part.astype(BF16).reshape(B, rows, pack * Rw)

    def tp_out(o, i, m):
        return remote(O.at[o, :, chunk(m)], tp_in.at[o, t], tS.at[o, i], tR.at[o, t], f, m)

    def tp_got(o, i, m):
        return remote(tp_in.at[o, m], tp_in.at[o, m], tS.at[o, i], tR.at[o, m], f, m)

    spread(1, 0)
    for i, m in enumerate(mates):
        tp_out(1, i, m).start()

    @pl.loop(0, Fs // wide)
    def _(c):
        at = pl.ds(pl.multiple_of(c * wide, wide), wide)
        positive = jnp.maximum(product(0, 0, at), 0.0)
        H[0, :, at] = (positive * positive).astype(BF16)

    spread(0, 1)
    for i, m in enumerate(mates):
        tp_out(0, i, m).start()

    def plane_out(o, i, q):
        return remote(S.at[o, q], pl_in.at[o, p], pS.at[o, i], pR.at[o, p], z * B + q, t)

    def plane_got(o, i, q):
        return remote(pl_in.at[o, q], pl_in.at[o, q], pS.at[o, i], pR.at[o, q], z * B + q, t)

    for o in (1, 0):
        for i, m in enumerate(mates):
            tp_got(o, i, m).wait_recv()
        for q in peers + [p]:
            total = O[o, q, chunk(t)].astype(F32)
            for m in mates:
                total = total + tp_in[o, m, q].astype(F32)
            S[o, q] = total.astype(BF16)
        for i, q in enumerate(peers):
            plane_out(o, i, q).start()

    for i in range(A - 1):
        right_d, left_d = A - 1 - i, i

        @pl.when(jnp.logical_and(has_left, z < right_d))
        def _(d=right_d):
            to_right(d).wait_recv()
            G[d] = (G[d].astype(F32) + from_left[d].astype(F32)).astype(BF16)
            to_right(d).start()

        @pl.when(jnp.logical_and(has_right, z > left_d))
        def _(d=left_d):
            remote(from_right.at[d], from_right.at[d], gS.at[d], gR.at[d], f, t).wait_recv()
            G[d] = (G[d].astype(F32) + from_right[d].astype(F32)).astype(BF16)
            to_left(d).start()

    outs = (out, ing)

    def share(o, i, m):
        there = outs[o].at[chunk(t)]
        return remote(there, there, fS.at[o, i], fR.at[o, t], f, m)

    def shared(o, i, m):
        there = outs[o].at[chunk(m)]
        return remote(there, there, fS.at[o, i], fR.at[o, m], f, m)

    for o in (1, 0):
        total = S[o, p].astype(F32)
        for i, q in enumerate(peers):
            plane_got(o, i, q).wait_recv()
            total = total + pl_in[o, q].astype(F32)
        outs[o][chunk(t)] = total.astype(BF16)
        for i, m in enumerate(mates):
            share(o, i, m).start()

    @pl.when(has_left)
    def _():
        remote(from_left.at[z], from_left.at[z], gS.at[z], gL.at[z], f, t).wait_recv()
        G[z] = (G[z].astype(F32) + from_left[z].astype(F32)).astype(BF16)

    @pl.when(has_right)
    def _():
        remote(from_right.at[z], from_right.at[z], gS.at[z], gR.at[z], f, t).wait_recv()
        G[z] = (G[z].astype(F32) + from_right[z].astype(F32)).astype(BF16)

    def grad_out(i, q):
        return remote(G.at[z, q], gout.at[p], hS.at[i], hR.at[p], z * B + q, t)

    for i, q in enumerate(peers):
        grad_out(i, q).start()
    gout[p] = G[z, p]

    for i, q in enumerate(peers):
        remote(gout.at[q], gout.at[q], hS.at[i], hR.at[q], z * B + q, t).wait_recv()
        grad_out(i, q).wait_send()
        for pc in range(2):
            slice_out(pc, i, q).wait_send()
        for j in range(3):
            act_out(j, i, q).wait_send()
        for o, m in enumerate(mates):
            act_share(i, q, o, m).wait_send()
        for o in range(2):
            plane_out(o, i, q).wait_send()
    for i, m in enumerate(mates):
        for o in range(2):
            tp_out(o, i, m).wait_send()
            share(o, i, m).wait_send()
            shared(o, i, m).wait_recv()
    for s in range(A):
        for pc in range(2):
            for q in range(B):

                @pl.when(jnp.logical_and(has_right, z >= s))
                def _(pc=pc, q=q, s=s):
                    line(pc, z - s, q, 0).wait_send()

                @pl.when(jnp.logical_and(has_left, z + s < A))
                def _(pc=pc, q=q, s=s):
                    line(pc, z + s, q, 1).wait_send()

    for d in range(A):

        @pl.when(z < d)
        def _(d=d):
            to_right(d).wait_send()

        @pl.when(z > d)
        def _(d=d):
            to_left(d).wait_send()


def groups(n, width):
    size = 1
    while 4 * size * size <= n and n % (2 * size) == 0 and width // (2 * size) >= 128:
        size *= 2
    return size


def per_device(n, T, fwd_input, saved_input, out_cotangent, up_weight, down_weight, up_grad_sum):
    rows, D = fwd_input.shape
    Rw, F = up_weight.shape
    B = groups(n, F)
    A, Fs, C = n // B, F // B, rows // T
    dma = pltpu.SemaphoreType.DMA
    side, mate = max(B - 1, 1), max(T - 1, 1)
    flops = 12 * B * rows * Fs * D
    vmem = pl.BlockSpec(memory_space=pltpu.VMEM)
    layer_out, input_grad, grad = pl.pallas_call(
        functools.partial(kernel, n, T, B),
        out_shape=(
            jax.ShapeDtypeStruct((rows, D), BF16),
            jax.ShapeDtypeStruct((rows, D), BF16),
            jax.ShapeDtypeStruct((B, Rw, Fs), BF16),
        ),
        in_specs=[vmem] * 5,
        out_specs=(vmem,) * 3,
        scratch_shapes=[
            pltpu.VMEM((3, B, rows, D), BF16),
            pltpu.VMEM((2, n, Rw, Fs), BF16),
            pltpu.VMEM((2, B * rows, Fs), BF16),
            pltpu.VMEM((2, B, rows, D), BF16),
            pltpu.VMEM((2, T, B, C, D), BF16),
            pltpu.VMEM((2, B, C, D), BF16),
            pltpu.VMEM((2, B, C, D), BF16),
            pltpu.VMEM((A, B, Rw, Fs), BF16),
            pltpu.VMEM((A, B, Rw, Fs), BF16),
            pltpu.VMEM((A, B, Rw, Fs), BF16),
            dma((5,)),
            dma((2, side)), dma((2, B)),
            dma((2, 2, n)), dma((2, n)),
            dma((3, side)), dma((3, B)),
            dma((side, mate)), dma((B, T)),
            dma((2, mate)), dma((2, T)),
            dma((2, side)), dma((2, B)),
            dma((2, mate)), dma((2, T)),
            dma((A,)), dma((A,)), dma((A,)),
            dma((side,)), dma((B,)),
        ],
        compiler_params=pltpu.CompilerParams(
            collective_id=0, has_side_effects=True, vmem_limit_bytes=58 * 2**20
        ),
        cost_estimate=pl.CostEstimate(flops=flops, bytes_accessed=2**25, transcendentals=0),
    )(fwd_input, saved_input, out_cotangent, up_weight, down_weight.T)
    grad_part = grad.astype(F32).transpose(1, 0, 2).reshape(Rw, F)
    grad_scale = float(rows * n) ** (-0.5)
    return (layer_out, input_grad, up_grad_sum + grad_part * grad_scale)


def solution(mesh):
    placed = (
        P("fs", None),
        P("fs", None),
        P("fs", None),
        P("fs", "tp"),
        P("tp", "fs"),
        P("fs", "tp"),
    )
    return jax.shard_map(
        functools.partial(per_device, mesh.shape["fs"], mesh.shape["tp"]),
        mesh=mesh,
        in_specs=placed,
        out_specs=(P("fs", None), P("fs", None), P("fs", "tp")),
        check_vma=False,
    )
```

time: 666 us -> 140 us (0.21)
  waiting for transfers between devices: 609 us -> 0 us
  Pallas kernels: 0 us -> 130 us
  matrix products: 33.4 us -> 0 us
  between operations: 13.8 us -> 0.68 us
    reduce_scatter x1 -> x0, waiting for transfers between devices: 339 us -> none  [per_device(): lax.psum_scatter(lax.dot_general(saved_input, d_pre, (((0,), (0,)), ((),...]
    all_gather x2 -> x0, waiting for transfers between devices: 249 us -> none  [the longest x1 135 us: per_device(): down_whole = lax.all_gather(down_weight, 'fs', axis=1, tiled=True)]
    pallas_call x0 -> x1, Pallas kernels: none -> 130 us  [per_device(): pl.pallas_call(functools.partial(kernel, n, T, B), out_shape=(jax.ShapeDt...]
    dot_general x5 -> x0, matrix products: 33.4 us -> none  [the longest x1 8.12 us: per_device(): lax.dot_general(saved_input, d_pre, (((0,), (0,)), ((), ())), preferred_e...]
    psum x1 -> x0, waiting for transfers between devices: 19.9 us -> none  [per_device(): layer_out = lax.psum(out_part.astype(jnp.bfloat16), 'tp')]
  transfers between devices with their start and end apart: 4 -> 0, of which waited for: 4 -> 0; matrix products, arithmetic and copies ran while one was open for 3% -> 0% of each run, Pallas kernels for 0% -> 0%
where the time goes in v1:
time: 140 us; the launch traced here: 139 us
  Pallas kernels  130 us (93%)
  local copies, waits for them, and re-layouts  7.26 us (5%)
    pallas_call x1, Pallas kernels, per_device(): pl.pallas_call(functools.partial(kernel, n, T, B), out_shape=(jax.ShapeDt...  130 us
    unnamed x9, local copies, waits for them, and re-layouts  6.93 us

profile of v1, /device:TPU:10, one launch (start us, length us, event | category | flops | bytes accessed | tf_op | source)
XLA Modules:
  0.0 139.3 jit_solution(18133057528194152631)
XLA Ops:
  0.6 2.0 %copy.10 = bf16[2048,128]{0,1:T(8,128)(2,1)} copy(bf16[2048,128]{1,0:T(8,128)(2,1)} %param.10) | data formatting | bytes 1048576 | tf_op args[4]
  2.7 130.1 %shard_map.85 = (bf16[128,2048]{1,0:T(8,128)(2,1)}, bf16[128,2048]{1,0:T(8,128)(2,1)}, bf16[4,128,512]{2,1,0:T(8,128)(2,1)}) custom-call(bf16[128,2048]{1,0:T(8,128)(2,1)} %fwd.1, bf16[128,2048]{1,0:T(8,128)(2,1)} %saved.1, bf16[128,2048]{1,0:T(8,128)(2,1)} %cot.1, bf16[128,2048]{1,0:T(8,128)(2,1)} %up.1, bf16[128,2048]{1,0:T(8,128)(2,1)} %bitcast.5), custom_call_target="tpu_custom_call" | custom-call | flops 6442450944 | bytes 33554432 | tf_op jit(solution)/shard_map/pallas_call | solution.py:367
  132.8 1.2 multiply_bitcast_fusion
  134.0 0.3 copy.11
  134.3 1.6 %copy.12 = f32[128,2048]{0,1:T(8,128)S(1)} copy(f32[128,2048]{1,0:T(8,128)} %param.11) | data formatting | bytes 2097152 | tf_op args[5]
  135.9 0.1 bitcast_add_fusion
  136.0 0.0 copy-start.1
  136.0 1.3 copy.13
  137.3 0.0 copy-done.1
  137.3 0.0 copy-start
  137.3 0.8 copy.16
  138.1 0.4 copy-done
  138.6 0.8 copy.17
Async XLA Ops:
  136.0 1.3 copy-start.1
  137.3 1.2 copy-start

commit v2 on v1

v2 whole, which is shorter than its diff:
```python
import functools

import jax
import jax.numpy as jnp
from jax import lax
from jax.experimental import pallas as pl
from jax.experimental.pallas import tpu as pltpu
from jax.sharding import PartitionSpec as P

MESH = pl.DeviceIdType.MESH
F32 = jnp.float32
BF16 = jnp.bfloat16
PART = 256


def remote(src, dst, send_sem, recv_sem, fs, tp):
    return pltpu.make_async_remote_copy(
        src_ref=src,
        dst_ref=dst,
        send_sem=send_sem,
        recv_sem=recv_sem,
        device_id=(fs, tp),
        device_id_type=MESH,
    )


def kernel(
    n, T, B, Q, fwd, saved, cot, up, down, out, ing, gout,
    X, W, turned, H, O, tp_in, S, pl_in, G, from_left, from_right,
    lsem, wS, wR, zS, zR, aS, aR, bS, bR, tS, tR, pS, pR, fS, fR, gS, gL, gR, hS, hR,
):
    A = n // B
    f, t = lax.axis_index("fs"), lax.axis_index("tp")
    z, p = lax.div(f, B), lax.rem(f, B)
    far = A - 1 - z
    rows, D = fwd.shape
    C = rows // T
    Rw, F = up.shape
    Fs = F // B
    wide = Fs // Q
    tokens = B * rows
    peers = [lax.rem(p + i, B) for i in range(1, B)]
    mates = [lax.rem(t + i, T) for i in range(1, T)]
    has_left, has_right = z > 0, z < A - 1

    def chunk(index):
        return pl.ds(pl.multiple_of(index * C, C), C)

    def cols(index, c):
        return pl.ds(pl.multiple_of(index * Fs + c * wide, wide), wide)

    barrier = pltpu.get_barrier_semaphore()
    for q in peers:
        pl.semaphore_signal(barrier, inc=1, device_id=(z * B + q, t), device_id_type=MESH)
    for m in mates:
        pl.semaphore_signal(barrier, inc=1, device_id=(f, m), device_id_type=MESH)

    @pl.when(has_left)
    def _():
        pl.semaphore_signal(barrier, inc=1, device_id=(f - B, t), device_id_type=MESH)

    @pl.when(has_right)
    def _():
        pl.semaphore_signal(barrier, inc=1, device_id=(f + B, t), device_id_type=MESH)

    ends = lax.div(z + A - 1, A) + lax.div(far + A - 1, A)
    pl.semaphore_wait(barrier, B - 1 + T - 1 + ends)

    weights = (up, down if down.shape == up.shape else turned)

    def slice_out(c, pc, i, q):
        return remote(
            weights[pc].at[:, cols(q, c)], W.at[c, pc, f], wS.at[c, pc, i], wR.at[c, pc, p], z * B + q, t
        )

    def slice_in(c, pc, q):
        there = W.at[c, pc, z * B + q]
        return remote(there, there, wS.at[c, pc, 0], wR.at[c, pc, q], z * B + q, t)

    def line(c, pc, k, q, way, src=None):
        at = k * B + q
        block = W.at[c, pc, at]
        target = f + B if way == 0 else f - B
        return remote(
            block if src is None else src, block, zS.at[way, c, pc, at], zR.at[c, pc, at], target, t
        )

    def own_out(c, pc, q, way):
        src = weights[pc].at[:, cols(p, c)] if q is p else None
        line(c, pc, z, q, way, src).start()

    def both_ways(c, pc, q):
        @pl.when(has_right)
        def _():
            own_out(c, pc, q, 0)

        @pl.when(has_left)
        def _():
            own_out(c, pc, q, 1)

    own_w = [
        pltpu.make_async_copy(weights[pc].at[:, cols(p, c)], W.at[c, pc, f], lsem.at[3 + 2 * c + pc])
        for c in range(Q) for pc in range(2)
    ]
    for c in range(Q):
        for pc in range(2):
            if (c, pc) == (0, 1) and weights[1] is turned:
                turned[...] = down[...].T
            for i, q in enumerate(peers):
                slice_out(c, pc, i, q).start()
            if c == 0:
                both_ways(c, pc, p)
    for copy in own_w:
        copy.start()

    acts = (fwd, saved, cot)

    def act_out(j, i, q):
        return remote(acts[j].at[chunk(t)], X.at[j, p, chunk(t)], aS.at[j, i], aR.at[j, p], z * B + q, t)

    def act_in(j, q):
        there = X.at[j, q, chunk(t)]
        return remote(there, there, aS.at[j, 0], aR.at[j, q], z * B + q, t)

    own_x = [pltpu.make_async_copy(acts[j], X.at[j, p], lsem.at[j]) for j in range(3)]
    for j in (1, 2, 0):
        own_x[j].start()
        for i, q in enumerate(peers):
            act_out(j, i, q).start()

    def act_share(i, q, o, m):
        there = X.at[:, q, chunk(t)]
        return remote(there, there, bS.at[i, o], bR.at[q, t], f, m)

    def act_shared(i, q, o, m):
        there = X.at[:, q, chunk(m)]
        return remote(there, there, bS.at[i, o], bR.at[q, m], f, m)

    for pc in range(2):
        for q in peers:
            slice_in(0, pc, q).wait_recv()
            both_ways(0, pc, q)

    order = [p] + peers

    def gather_step(c, s):
        for pc in range(2):
            for q in order:

                @pl.when(z >= s)
                def _(pc=pc, q=q):
                    line(c, pc, z - s, q, 0).wait_recv()

                    @pl.when(has_right)
                    def _():
                        line(c, pc, z - s, q, 0).start()

                @pl.when(far >= s)
                def _(pc=pc, q=q):
                    line(c, pc, z + s, q, 1).wait_recv()

                    @pl.when(has_left)
                    def _():
                        line(c, pc, z + s, q, 1).start()

        if c == 0 and s == 1:
            for later in range(1, Q):
                for pc in range(2):
                    for q in peers:
                        slice_in(later, pc, q).wait_recv()
        if c + 1 < Q:
            @pl.when(jnp.logical_and(has_right, z == s if s > 1 else z <= 1))
            def _():
                for pc in range(2):
                    for q in order:
                        own_out(c + 1, pc, q, 0)

            @pl.when(jnp.logical_and(has_left, far == s if s > 1 else far <= 1))
            def _():
                for pc in range(2):
                    for q in order:
                        own_out(c + 1, pc, q, 1)

        if c == 0 and s == max(A - 2, 1):
            for i, q in enumerate(peers):
                for j in range(3):
                    act_in(j, q).wait_recv()
                for o, m in enumerate(mates):
                    act_share(i, q, o, m).start()

    def product(c, j, pc):
        return jnp.dot(
            X[j].reshape(tokens, D), W[c, pc].reshape(D, wide), preferred_element_type=F32
        )

    def to_right(c, d):
        return remote(G.at[c, d], from_left.at[c, d], gS.at[c, d], gL.at[c, d], f + B, t)

    def to_left(c, d):
        return remote(G.at[c, d], from_right.at[c, d], gS.at[c, d], gR.at[c, d], f - B, t)

    def add_left(c, d):
        remote(from_left.at[c, d], from_left.at[c, d], gS.at[c, d], gL.at[c, d], f - B, t).wait_recv()
        G[c, d] = (G[c, d].astype(F32) + from_left[c, d].astype(F32)).astype(BF16)

    def add_right(c, d):
        remote(from_right.at[c, d], from_right.at[c, d], gS.at[c, d], gR.at[c, d], f + B, t).wait_recv()
        G[c, d] = (G[c, d].astype(F32) + from_right[c, d].astype(F32)).astype(BF16)

    def grad_out(c, i, q):
        return remote(G.at[c, z, q], gout.at[:, cols(p, c)], hS.at[c, i], hR.at[c, p], z * B + q, t)

    def sum_step(c, s):
        if s < A - 1:

            @pl.when(jnp.logical_and(has_left, z <= s))
            def _():
                add_left(c, far - s + 2 * z)
                to_right(c, far - s + 2 * z).start()

            @pl.when(jnp.logical_and(has_right, far <= s))
            def _():
                add_right(c, s - far)
                to_left(c, s - far).start()

        else:

            @pl.when(has_left)
            def _():
                add_left(c, z)

            @pl.when(has_right)
            def _():
                add_right(c, z)

            for i, q in enumerate(peers):
                grad_out(c, i, q).start()
            gout[:, cols(p, c)] = G[c, z, p]

    planes = []
    for i in range((A + 1) // 2):
        planes += [A - 1 - i] if A - 1 - i == i else [A - 1 - i, i]
    deep = B * Rw

    def backward(c):
        pre = product(c, 1, 0)
        d_hidden = product(c, 2, 1)
        H[1, c] = (d_hidden * 2.0 * jnp.maximum(pre, 0.0)).astype(BF16)
        for d in planes:
            term = lax.dot_general(
                X[1, :, :, d * deep:(d + 1) * deep].reshape(tokens, deep),
                H[1, c],
                (((0,), (0,)), ((), ())),
                preferred_element_type=F32,
            )
            G[c, d] = term.astype(BF16).reshape(B, Rw, wide)
            if d > 0:

                @pl.when(z == 0)
                def _(d=d):
                    to_right(c, d).start()

            if d < A - 1:

                @pl.when(far == 0)
                def _(d=d):
                    to_left(c, d).start()

    def forward(c):
        positive = jnp.maximum(product(c, 0, 0), 0.0)
        H[0, c] = (positive * positive).astype(BF16)

    for c in range(Q):
        for s in range(1, A):
            gather_step(c, s)
            if c > 0:
                sum_step(c - 1, s)
        if c == 0:
            for copy in own_w + own_x:
                copy.wait()
            for i, q in enumerate(peers):
                for o, m in enumerate(mates):
                    act_shared(i, q, o, m).wait_recv()
        backward(c)
        if c + 1 < Q:
            forward(c)

    pack = max(1, 256 // Rw)

    def spread(o, pc):
        @pl.loop(0, n // pack)
        def _(g):
            part = 0.0
            for c in range(Q):
                block = W[c, pc, pl.ds(g * pack, pack)].reshape(pack * Rw, wide)
                part += lax.dot_general(
                    H[o, c], block, (((1,), (1,)), ((), ())), preferred_element_type=F32
                )
            at = pl.ds(pl.multiple_of(g * (pack * Rw), pack * Rw), pack * Rw)
            O[o, :, :, at] = part.astype(BF16).reshape(B, rows, pack * Rw)

    def tp_out(o, i, m):
        return remote(O.at[o, :, chunk(m)], tp_in.at[o, t], tS.at[o, i], tR.at[o, t], f, m)

    def tp_got(o, i, m):
        return remote(tp_in.at[o, m], tp_in.at[o, m], tS.at[o, i], tR.at[o, m], f, m)

    def plane_out(o, i, q):
        return remote(S.at[o, q], pl_in.at[o, p], pS.at[o, i], pR.at[o, p], z * B + q, t)

    def plane_got(o, i, q):
        return remote(pl_in.at[o, q], pl_in.at[o, q], pS.at[o, i], pR.at[o, q], z * B + q, t)

    def plane_sums(o):
        for i, m in enumerate(mates):
            tp_got(o, i, m).wait_recv()
        for i, q in enumerate(peers + [p]):
            total = O[o, q, chunk(t)].astype(F32)
            for m in mates:
                total = total + tp_in[o, m, q].astype(F32)
            S[o, q] = total.astype(BF16)
            if i < len(peers):
                plane_out(o, i, q).start()

    spread(1, 0)
    for i, m in enumerate(mates):
        tp_out(1, i, m).start()
    forward(Q - 1)
    plane_sums(1)
    spread(0, 1)
    for i, m in enumerate(mates):
        tp_out(0, i, m).start()
    plane_sums(0)
    for s in range(1, A):
        sum_step(Q - 1, s)

    outs = (out, ing)

    def share(o, i, m):
        there = outs[o].at[chunk(t)]
        return remote(there, there, fS.at[o, i], fR.at[o, t], f, m)

    def shared(o, i, m):
        there = outs[o].at[chunk(m)]
        return remote(there, there, fS.at[o, i], fR.at[o, m], f, m)

    for o in (1, 0):
        total = S[o, p].astype(F32)
        for i, q in enumerate(peers):
            plane_got(o, i, q).wait_recv()
            total = total + pl_in[o, q].astype(F32)
        outs[o][chunk(t)] = total.astype(BF16)
        for i, m in enumerate(mates):
            share(o, i, m).start()

    for i, q in enumerate(peers):
        for c in range(Q):
            there = gout.at[:, cols(q, c)]
            remote(there, there, hS.at[c, i], hR.at[c, q], z * B + q, t).wait_recv()
            grad_out(c, i, q).wait_send()
            for pc in range(2):
                slice_out(c, pc, i, q).wait_send()
        for j in range(3):
            act_out(j, i, q).wait_send()
        for o, m in enumerate(mates):
            act_share(i, q, o, m).wait_send()
        for o in range(2):
            plane_out(o, i, q).wait_send()
    for i, m in enumerate(mates):
        for o in range(2):
            tp_out(o, i, m).wait_send()
            share(o, i, m).wait_send()
            shared(o, i, m).wait_recv()
    for s in range(A):

        @pl.when(jnp.logical_and(has_right, z >= s))
        def _(s=s):
            for c in range(Q):
                for pc in range(2):
                    for q in range(B):
                        line(c, pc, z - s, q, 0).wait_send()

        @pl.when(jnp.logical_and(has_left, far >= s))
        def _(s=s):
            for c in range(Q):
                for pc in range(2):
                    for q in range(B):
                        line(c, pc, z + s, q, 1).wait_send()

    for d in range(A):
        for c in range(Q):

            @pl.when(z < d)
            def _(c=c, d=d):
                to_right(c, d).wait_send()

            @pl.when(z > d)
            def _(c=c, d=d):
                to_left(c, d).wait_send()


def groups(n, width):
    size = 1
    while 4 * size * size <= n and n % (2 * size) == 0 and width // (2 * size) >= 128:
        size *= 2
    return size


def per_device(n, T, fwd_input, saved_input, out_cotangent, up_weight, down_weight, up_grad_sum):
    rows, D = fwd_input.shape
    Rw, F = up_weight.shape
    B = groups(n, F)
    A, Fs, C = n // B, F // B, rows // T
    Q = max(1, Fs // PART)
    wide = Fs // Q
    down = down_weight if Rw % 128 == 0 and down_weight.shape != up_weight.shape else down_weight.T
    dma = pltpu.SemaphoreType.DMA
    side, mate = max(B - 1, 1), max(T - 1, 1)
    flops = 12 * B * rows * Fs * D
    vmem = pl.BlockSpec(memory_space=pltpu.VMEM)
    layer_out, input_grad, grad = pl.pallas_call(
        functools.partial(kernel, n, T, B, Q),
        out_shape=(
            jax.ShapeDtypeStruct((rows, D), BF16),
            jax.ShapeDtypeStruct((rows, D), BF16),
            jax.ShapeDtypeStruct((Rw, F), BF16),
        ),
        in_specs=[vmem] * 5,
        out_specs=(vmem,) * 3,
        scratch_shapes=[
            pltpu.VMEM((3, B, rows, D), BF16),
            pltpu.VMEM((Q, 2, n, Rw, wide), BF16),
            pltpu.VMEM((Rw, F), BF16),
            pltpu.VMEM((2, Q, B * rows, wide), BF16),
            pltpu.VMEM((2, B, rows, D), BF16),
            pltpu.VMEM((2, T, B, C, D), BF16),
            pltpu.VMEM((2, B, C, D), BF16),
            pltpu.VMEM((2, B, C, D), BF16),
            pltpu.VMEM((Q, A, B, Rw, wide), BF16),
            pltpu.VMEM((Q, A, B, Rw, wide), BF16),
            pltpu.VMEM((Q, A, B, Rw, wide), BF16),
            dma((3 + 2 * Q,)),
            dma((Q, 2, side)), dma((Q, 2, B)),
            dma((2, Q, 2, n)), dma((Q, 2, n)),
            dma((3, side)), dma((3, B)),
            dma((side, mate)), dma((B, T)),
            dma((2, mate)), dma((2, T)),
            dma((2, side)), dma((2, B)),
            dma((2, mate)), dma((2, T)),
            dma((Q, A)), dma((Q, A)), dma((Q, A)),
            dma((Q, side)), dma((Q, B)),
        ],
        compiler_params=pltpu.CompilerParams(
            collective_id=0, has_side_effects=True, vmem_limit_bytes=58 * 2**20
        ),
        cost_estimate=pl.CostEstimate(flops=flops, bytes_accessed=2**25, transcendentals=0),
    )(fwd_input, saved_input, out_cotangent, up_weight, down)
    grad_part = grad.astype(F32)
    grad_scale = float(rows * n) ** (-0.5)
    return (layer_out, input_grad, up_grad_sum + grad_part * grad_scale)


def solution(mesh):
    placed = (
        P("fs", None),
        P("fs", None),
        P("fs", None),
        P("fs", "tp"),
        P("tp", "fs"),
        P("fs", "tp"),
    )
    return jax.shard_map(
        functools.partial(per_device, mesh.shape["fs"], mesh.shape["tp"]),
        mesh=mesh,
        in_specs=placed,
        out_specs=(P("fs", None), P("fs", None), P("fs", "tp")),
        check_vma=False,
    )
```

time: 140 us -> 135 us (0.964)
  the two profiles are of different devices: /device:TPU:10 before, /device:TPU:0 now
where the time goes in v2:
time: 135 us
  Pallas kernels  130 us (96%)
  other arithmetic  2.2 us (2%)
  local copies, waits for them, and re-layouts  2.03 us (2%)
    pallas_call x1, Pallas kernels, per_device(): pl.pallas_call(functools.partial(kernel, n, T, B, Q), out_shape=(jax.Shap...  130 us

profile of v2, /device:TPU:0, one launch (start us, length us, event | category | flops | bytes accessed | tf_op | source)
XLA Modules:
  0.0 134.5 jit_solution(864883186087772867)
XLA Ops:
  0.6 0.0 copy-start
  0.6 129.6 %shard_map.85 = (bf16[128,2048]{1,0:T(8,128)(2,1)}, bf16[128,2048]{1,0:T(8,128)(2,1)}, bf16[128,2048]{1,0:T(8,128)(2,1)}) custom-call(bf16[128,2048]{1,0:T(8,128)(2,1)} %fwd.1, bf16[128,2048]{1,0:T(8,128)(2,1)} %saved.1, bf16[128,2048]{1,0:T(8,128)(2,1)} %cot.1, bf16[128,2048]{1,0:T(8,128)(2,1)} %up.1, bf16[2048,128]{1,0:T(8,128)(2,1)} %down.1), custom_call_target="tpu_custom_call" | custom-call | flops 6442450944 | bytes 33554432 | tf_op jit(solution)/shard_map/pallas_call | solution.py:421
  130.3 0.0 copy-done
  130.3 0.0 copy-start.2
  130.3 2.2 %multiply_add_fusion = f32[128,2048]{1,0:T(8,128)} fusion(f32[128,2048]{1,0:T(8,128)S(1)} %copy-done, bf16[128,2048]{1,0:T(8,128)(2,1)} %get-tuple-element.8), kind=kLoop, calls=%fused_computation | loop fusion | flops 786432 | bytes 2621440 | tf_op jit(solution)/shard_map/add | solution.py:460
  132.5 0.0 copy-done.2
  132.5 0.0 copy-start.1
  132.5 0.8 copy.11
  133.3 0.4 copy-done.1
  133.7 0.8 copy.12
Async XLA Ops:
  0.6 129.7 %copy-start = (f32[128,2048]{1,0:T(8,128)S(1)}, f32[128,2048]{1,0:T(8,128)}, u32[]{:S(2)}) copy-start(f32[128,2048]{1,0:T(8,128)} %param.11) | copy-start | bytes 3145732
  130.3 2.2 %copy-start.2 = (bf16[128,2048]{1,0:T(8,128)(2,1)S(1)}, bf16[128,2048]{1,0:T(8,128)(2,1)}, u32[]{:S(2)}) copy-start(bf16[128,2048]{1,0:T(8,128)(2,1)} %get-tuple-element.12) | copy-start | bytes 1572868
  132.5 1.2 copy-start.1

commit v3 on v2

--- a/solution.py
+++ b/solution.py
@@ -26,7 +26,7 @@
 
 def kernel(
     n, T, B, Q, fwd, saved, cot, up, down, out, ing, gout,
-    X, W, turned, H, O, tp_in, S, pl_in, G, from_left, from_right,
+    X, W, turned, H, pre, O, tp_in, S, pl_in, G, from_left, from_right,
     lsem, wS, wR, zS, zR, aS, aR, bS, bR, tS, tR, pS, pR, fS, fR, gS, gL, gR, hS, hR,
 ):
     A = n // B
@@ -42,6 +42,8 @@
     peers = [lax.rem(p + i, B) for i in range(1, B)]
     mates = [lax.rem(t + i, T) for i in range(1, T)]
     has_left, has_right = z > 0, z < A - 1
+    stages = [(c, pc) for pc in range(2) for c in range(Q)]
+    last = len(stages) - 1
 
     def chunk(index):
         return pl.ds(pl.multiple_of(index * C, C), C)
@@ -100,16 +102,15 @@
 
     own_w = [
         pltpu.make_async_copy(weights[pc].at[:, cols(p, c)], W.at[c, pc, f], lsem.at[3 + 2 * c + pc])
-        for c in range(Q) for pc in range(2)
+        for c, pc in stages
     ]
-    for c in range(Q):
-        for pc in range(2):
-            if (c, pc) == (0, 1) and weights[1] is turned:
-                turned[...] = down[...].T
-            for i, q in enumerate(peers):
-                slice_out(c, pc, i, q).start()
-            if c == 0:
-                both_ways(c, pc, p)
+    for c, pc in stages:
+        if (c, pc) == (0, 1) and weights[1] is turned:
+            turned[...] = down[...].T
+        for i, q in enumerate(peers):
+            slice_out(c, pc, i, q).start()
+        if (c, pc) == stages[0]:
+            both_ways(c, pc, p)
     for copy in own_w:
         copy.start()
 
@@ -136,52 +137,48 @@
         there = X.at[:, q, chunk(m)]
         return remote(there, there, bS.at[i, o], bR.at[q, m], f, m)
 
-    for pc in range(2):
-        for q in peers:
-            slice_in(0, pc, q).wait_recv()
-            both_ways(0, pc, q)
+    for q in peers:
+        slice_in(0, 0, q).wait_recv()
+        both_ways(0, 0, q)
 
     order = [p] + peers
 
-    def gather_step(c, s):
-        for pc in range(2):
-            for q in order:
-
-                @pl.when(z >= s)
-                def _(pc=pc, q=q):
-                    line(c, pc, z - s, q, 0).wait_recv()
-
-                    @pl.when(has_right)
-                    def _():
-                        line(c, pc, z - s, q, 0).start()
-
-                @pl.when(far >= s)
-                def _(pc=pc, q=q):
-                    line(c, pc, z + s, q, 1).wait_recv()
-
-                    @pl.when(has_left)
-                    def _():
-                        line(c, pc, z + s, q, 1).start()
-
-        if c == 0 and s == 1:
-            for later in range(1, Q):
-                for pc in range(2):
-                    for q in peers:
-                        slice_in(later, pc, q).wait_recv()
-        if c + 1 < Q:
+    def gather_step(stage, s):
+        c, pc = stages[stage]
+        for q in order:
+
+            @pl.when(z >= s)
+            def _(q=q):
+                line(c, pc, z - s, q, 0).wait_recv()
+
+                @pl.when(has_right)
+                def _():
+                    line(c, pc, z - s, q, 0).start()
+
+            @pl.when(far >= s)
+            def _(q=q):
+                line(c, pc, z + s, q, 1).wait_recv()
+
+                @pl.when(has_left)
+                def _():
+                    line(c, pc, z + s, q, 1).start()
+
+        if stage == 0 and s == 1:
+            for later in stages[1:]:
+                for q in peers:
+                    slice_in(*later, q).wait_recv()
+        if stage < last:
             @pl.when(jnp.logical_and(has_right, z == s if s > 1 else z <= 1))
             def _():
-                for pc in range(2):
-                    for q in order:
-                        own_out(c + 1, pc, q, 0)
+                for q in order:
+                    own_out(*stages[stage + 1], q, 0)
 
             @pl.when(jnp.logical_and(has_left, far == s if s > 1 else far <= 1))
             def _():
-                for pc in range(2):
-                    for q in order:
-                        own_out(c + 1, pc, q, 1)
-
-        if c == 0 and s == max(A - 2, 1):
+                for q in order:
+                    own_out(*stages[stage + 1], q, 1)
+
+        if stage == last - 1 and s == 1:
             for i, q in enumerate(peers):
                 for j in range(3):
                     act_in(j, q).wait_recv()
@@ -243,9 +240,8 @@
     deep = B * Rw
 
     def backward(c):
-        pre = product(c, 1, 0)
         d_hidden = product(c, 2, 1)
-        H[1, c] = (d_hidden * 2.0 * jnp.maximum(pre, 0.0)).astype(BF16)
+        H[1, c] = (d_hidden * 2.0 * jnp.maximum(pre[c], 0.0)).astype(BF16)
         for d in planes:
             term = lax.dot_general(
                 X[1, :, :, d * deep:(d + 1) * deep].reshape(tokens, deep),
@@ -269,68 +265,94 @@
     def forward(c):
         positive = jnp.maximum(product(c, 0, 0), 0.0)
         H[0, c] = (positive * positive).astype(BF16)
-
-    for c in range(Q):
+        pre[c] = product(c, 1, 0)
+
+    def columns(k):
+        return pl.ds(pl.multiple_of(k * deep, deep), deep)
+
+    def tp_out(o, i, m, k):
+        return remote(
+            O.at[o, :, chunk(m), columns(k)], tp_in.at[o, t, :, :, columns(k)],
+            tS.at[o, i, k], tR.at[o, t, k], f, m,
+        )
+
+    def tp_got(o, i, m, k):
+        there = tp_in.at[o, m, :, :, columns(k)]
+        return remote(there, there, tS.at[o, i, k], tR.at[o, m, k], f, m)
+
+    def plane_out(o, i, q, k):
+        return remote(
+            S.at[o, q, :, columns(k)], pl_in.at[o, p, :, columns(k)],
+            pS.at[o, i, k], pR.at[o, p, k], z * B + q, t,
+        )
+
+    def plane_got(o, i, q, k):
+        there = pl_in.at[o, q, :, columns(k)]
+        return remote(there, there, pS.at[o, i, k], pR.at[o, q, k], z * B + q, t)
+
+    def spread(o, pc, k):
+        part = 0.0
+        for c in range(Q):
+            block = W[c, pc, pl.ds(k * B, B)].reshape(deep, wide)
+            part += lax.dot_general(
+                H[o, c], block, (((1,), (1,)), ((), ())), preferred_element_type=F32
+            )
+        O[o, :, :, columns(k)] = part.astype(BF16).reshape(B, rows, deep)
+        for i, m in enumerate(mates):
+            tp_out(o, i, m, k).start()
+
+    def plane_sums(o, k):
+        for i, m in enumerate(mates):
+            tp_got(o, i, m, k).wait_recv()
+        for i, q in enumerate(peers + [p]):
+            total = O[o, q, chunk(t), columns(k)].astype(F32)
+            for m in mates:
+                total = total + tp_in[o, m, q, :, columns(k)].astype(F32)
+            S[o, q, :, columns(k)] = total.astype(BF16)
+            if i < len(peers):
+                plane_out(o, i, q, k).start()
+
+    def out_step(s, work):
+        if s == 0:
+            work(z)
+            return
+
+        @pl.when(z >= s)
+        def _():
+            work(z - s)
+
+        @pl.when(far >= s)
+        def _():
+            work(z + s)
+
+    for stage in range(last + 1):
+        c = stage - Q
         for s in range(1, A):
-            gather_step(c, s)
+            if stage == last:
+                out_step(s - 1, lambda k: spread(0, 1, k))
+            gather_step(stage, s)
             if c > 0:
                 sum_step(c - 1, s)
-        if c == 0:
+            if stage == last:
+                out_step(s - 1, lambda k: plane_sums(0, k))
+        if stage == last - 1:
             for copy in own_w + own_x:
                 copy.wait()
             for i, q in enumerate(peers):
                 for o, m in enumerate(mates):
                     act_shared(i, q, o, m).wait_recv()
-        backward(c)
-        if c + 1 < Q:
-            forward(c)
-
-    pack = max(1, 256 // Rw)
-
-    def spread(o, pc):
-        @pl.loop(0, n // pack)
-        def _(g):
-            part = 0.0
-            for c in range(Q):
-                block = W[c, pc, pl.ds(g * pack, pack)].reshape(pack * Rw, wide)
-                part += lax.dot_general(
-                    H[o, c], block, (((1,), (1,)), ((), ())), preferred_element_type=F32
-                )
-            at = pl.ds(pl.multiple_of(g * (pack * Rw), pack * Rw), pack * Rw)
-            O[o, :, :, at] = part.astype(BF16).reshape(B, rows, pack * Rw)
-
-    def tp_out(o, i, m):
-        return remote(O.at[o, :, chunk(m)], tp_in.at[o, t], tS.at[o, i], tR.at[o, t], f, m)
-
-    def tp_got(o, i, m):
-        return remote(tp_in.at[o, m], tp_in.at[o, m], tS.at[o, i], tR.at[o, m], f, m)
-
-    def plane_out(o, i, q):
-        return remote(S.at[o, q], pl_in.at[o, p], pS.at[o, i], pR.at[o, p], z * B + q, t)
-
-    def plane_got(o, i, q):
-        return remote(pl_in.at[o, q], pl_in.at[o, q], pS.at[o, i], pR.at[o, q], z * B + q, t)
-
-    def plane_sums(o):
-        for i, m in enumerate(mates):
-            tp_got(o, i, m).wait_recv()
-        for i, q in enumerate(peers + [p]):
-            total = O[o, q, chunk(t)].astype(F32)
-            for m in mates:
-                total = total + tp_in[o, m, q].astype(F32)
-            S[o, q] = total.astype(BF16)
-            if i < len(peers):
-                plane_out(o, i, q).start()
-
-    spread(1, 0)
-    for i, m in enumerate(mates):
-        tp_out(1, i, m).start()
-    forward(Q - 1)
-    plane_sums(1)
-    spread(0, 1)
-    for i, m in enumerate(mates):
-        tp_out(0, i, m).start()
-    plane_sums(0)
+            for part in range(Q):
+                forward(part)
+        if c >= 0:
+            backward(c)
+
+    spread(1, 0, 0)
+    for k in range(1, A):
+        spread(1, 0, k)
+        plane_sums(1, k - 1)
+    out_step(A - 1, lambda k: spread(0, 1, k))
+    plane_sums(1, A - 1)
+    out_step(A - 1, lambda k: plane_sums(0, k))
     for s in range(1, A):
         sum_step(Q - 1, s)
 
@@ -344,10 +366,11 @@
         there = outs[o].at[chunk(m)]
         return remote(there, there, fS.at[o, i], fR.at[o, m], f, m)
 
-    for o in (1, 0):
+    for o in (0, 1):
         total = S[o, p].astype(F32)
         for i, q in enumerate(peers):
-            plane_got(o, i, q).wait_recv()
+            for k in range(A):
+                plane_got(o, i, q, k).wait_recv()
             total = total + pl_in[o, q].astype(F32)
         outs[o][chunk(t)] = total.astype(BF16)
         for i, m in enumerate(mates):
@@ -365,10 +388,12 @@
         for o, m in enumerate(mates):
             act_share(i, q, o, m).wait_send()
         for o in range(2):
-            plane_out(o, i, q).wait_send()
+            for k in range(A):
+                plane_out(o, i, q, k).wait_send()
     for i, m in enumerate(mates):
         for o in range(2):
-            tp_out(o, i, m).wait_send()
+            for k in range(A):
+                tp_out(o, i, m, k).wait_send()
             share(o, i, m).wait_send()
             shared(o, i, m).wait_recv()
     for s in range(A):
@@ -432,6 +457,7 @@
             pltpu.VMEM((Q, 2, n, Rw, wide), BF16),
             pltpu.VMEM((Rw, F), BF16),
             pltpu.VMEM((2, Q, B * rows, wide), BF16),
+            pltpu.VMEM((Q, B * rows, wide), F32),
             pltpu.VMEM((2, B, rows, D), BF16),
             pltpu.VMEM((2, T, B, C, D), BF16),
             pltpu.VMEM((2, B, C, D), BF16),
@@ -444,8 +470,8 @@
             dma((2, Q, 2, n)), dma((Q, 2, n)),
             dma((3, side)), dma((3, B)),
             dma((side, mate)), dma((B, T)),
-            dma((2, mate)), dma((2, T)),
-            dma((2, side)), dma((2, B)),
+            dma((2, mate, A)), dma((2, T, A)),
+            dma((2, side, A)), dma((2, B, A)),
             dma((2, mate)), dma((2, T)),
             dma((Q, A)), dma((Q, A)), dma((Q, A)),
             dma((Q, side)), dma((Q, B)),

time: 135 us -> 123 us (0.911)
  the two profiles are of different devices: /device:TPU:0 before, /device:TPU:10 now
where the time goes in v3:
time: 123 us; the launch traced here: 122 us
  Pallas kernels  118 us (96%)
  other arithmetic  2.2 us (2%)
  local copies, waits for them, and re-layouts  2.03 us (2%)
    pallas_call x1, Pallas kernels, per_device(): pl.pallas_call(functools.partial(kernel, n, T, B, Q), out_shape=(jax.Shap...  118 us

profile of v3, /device:TPU:10, one launch (start us, length us, event | category | flops | bytes accessed | tf_op | source)
XLA Modules:
  0.0 122.4 jit_solution(16526203391430940368)
XLA Ops:
  0.6 0.0 copy-start
  0.6 117.5 %shard_map.85 = (bf16[128,2048]{1,0:T(8,128)(2,1)}, bf16[128,2048]{1,0:T(8,128)(2,1)}, bf16[128,2048]{1,0:T(8,128)(2,1)}) custom-call(bf16[128,2048]{1,0:T(8,128)(2,1)} %fwd.1, bf16[128,2048]{1,0:T(8,128)(2,1)} %saved.1, bf16[128,2048]{1,0:T(8,128)(2,1)} %cot.1, bf16[128,2048]{1,0:T(8,128)(2,1)} %up.1, bf16[2048,128]{1,0:T(8,128)(2,1)} %down.1), custom_call_target="tpu_custom_call" | custom-call | flops 6442450944 | bytes 33554432 | tf_op jit(solution)/shard_map/pallas_call | solution.py:446
  118.2 0.0 copy-done
  118.2 0.0 copy-start.2
  118.2 2.2 %multiply_add_fusion = f32[128,2048]{1,0:T(8,128)} fusion(f32[128,2048]{1,0:T(8,128)S(1)} %copy-done, bf16[128,2048]{1,0:T(8,128)(2,1)} %get-tuple-element.8), kind=kLoop, calls=%fused_computation | loop fusion | flops 786432 | bytes 2621440 | tf_op jit(solution)/shard_map/add | solution.py:486
  120.4 0.0 copy-done.2
  120.4 0.0 copy-start.1
  120.4 0.8 copy.11
  121.2 0.4 copy-done.1
  121.6 0.8 copy.12
Async XLA Ops:
  0.6 117.6 %copy-start = (f32[128,2048]{1,0:T(8,128)S(1)}, f32[128,2048]{1,0:T(8,128)}, u32[]{:S(2)}) copy-start(f32[128,2048]{1,0:T(8,128)} %param.11) | copy-start | bytes 3145732
  118.2 2.2 %copy-start.2 = (bf16[128,2048]{1,0:T(8,128)(2,1)S(1)}, bf16[128,2048]{1,0:T(8,128)(2,1)}, u32[]{:S(2)}) copy-start(bf16[128,2048]{1,0:T(8,128)(2,1)} %get-tuple-element.12) | copy-start | bytes 1572868
  120.4 1.2 %copy-start.1 = (bf16[128,2048]{1,0:T(8,128)(2,1)S(1)}, bf16[128,2048]{1,0:T(8,128)(2,1)}, u32[]{:S(2)}) copy-start(bf16[128,2048]{1,0:T(8,128)(2,1)} %get-tuple-element.13) | copy-start | bytes 1572868

commit v4 on v3

--- a/solution.py
+++ b/solution.py
@@ -81,14 +81,14 @@
 
     def line(c, pc, k, q, way, src=None):
         at = k * B + q
-        block = W.at[c, pc, at]
+        block = W.at[c, pc, at] if (c, pc) == stages[0] else W.at[c, pc, pl.ds(at, B)]
         target = f + B if way == 0 else f - B
         return remote(
             block if src is None else src, block, zS.at[way, c, pc, at], zR.at[c, pc, at], target, t
         )
 
     def own_out(c, pc, q, way):
-        src = weights[pc].at[:, cols(p, c)] if q is p else None
+        src = weights[pc].at[:, cols(p, c)] if q is p and (c, pc) == stages[0] else None
         line(c, pc, z, q, way, src).start()
 
     def both_ways(c, pc, q):
@@ -145,7 +145,7 @@
 
     def gather_step(stage, s):
         c, pc = stages[stage]
-        for q in order:
+        for q in order if stage == 0 else (0,):
 
             @pl.when(z >= s)
             def _(q=q):
@@ -167,16 +167,16 @@
             for later in stages[1:]:
                 for q in peers:
                     slice_in(*later, q).wait_recv()
+            for copy in own_w:
+                copy.wait()
         if stage < last:
             @pl.when(jnp.logical_and(has_right, z == s if s > 1 else z <= 1))
             def _():
-                for q in order:
-                    own_out(*stages[stage + 1], q, 0)
+                own_out(*stages[stage + 1], 0, 0)
 
             @pl.when(jnp.logical_and(has_left, far == s if s > 1 else far <= 1))
             def _():
-                for q in order:
-                    own_out(*stages[stage + 1], q, 1)
+                own_out(*stages[stage + 1], 0, 1)
 
         if stage == last - 1 and s == 1:
             for i, q in enumerate(peers):
@@ -336,7 +336,7 @@
             if stage == last:
                 out_step(s - 1, lambda k: plane_sums(0, k))
         if stage == last - 1:
-            for copy in own_w + own_x:
+            for copy in own_x:
                 copy.wait()
             for i, q in enumerate(peers):
                 for o, m in enumerate(mates):
@@ -352,8 +352,9 @@
         plane_sums(1, k - 1)
     out_step(A - 1, lambda k: spread(0, 1, k))
     plane_sums(1, A - 1)
+    sum_step(Q - 1, 1)
     out_step(A - 1, lambda k: plane_sums(0, k))
-    for s in range(1, A):
+    for s in range(2, A):
         sum_step(Q - 1, s)
 
     outs = (out, ing)
@@ -402,14 +403,14 @@
         def _(s=s):
             for c in range(Q):
                 for pc in range(2):
-                    for q in range(B):
+                    for q in range(B if (c, pc) == stages[0] else 1):
                         line(c, pc, z - s, q, 0).wait_send()
 
         @pl.when(jnp.logical_and(has_left, far >= s))
         def _(s=s):
             for c in range(Q):
                 for pc in range(2):
-                    for q in range(B):
+                    for q in range(B if (c, pc) == stages[0] else 1):
                         line(c, pc, z + s, q, 1).wait_send()
 
     for d in range(A):

time: 123 us -> 123 us (level)
  no operation moved by 1% of the time
where the time goes in v4:
time: 123 us; the launch traced here: 122 us
  Pallas kernels  117 us (95%)
  other arithmetic  2.2 us (2%)
  local copies, waits for them, and re-layouts  2.03 us (2%)
    pallas_call x1, Pallas kernels, per_device(): pl.pallas_call(functools.partial(kernel, n, T, B, Q), out_shape=(jax.Shap...  117 us

profile of v4, /device:TPU:10, one launch (start us, length us, event | category | flops | bytes accessed | tf_op | source)
XLA Modules:
  0.0 122.3 jit_solution(15751235714993204141)
XLA Ops:
  0.6 0.0 copy-start
  0.6 117.4 %shard_map.85 = (bf16[128,2048]{1,0:T(8,128)(2,1)}, bf16[128,2048]{1,0:T(8,128)(2,1)}, bf16[128,2048]{1,0:T(8,128)(2,1)}) custom-call(bf16[128,2048]{1,0:T(8,128)(2,1)} %fwd.1, bf16[128,2048]{1,0:T(8,128)(2,1)} %saved.1, bf16[128,2048]{1,0:T(8,128)(2,1)} %cot.1, bf16[128,2048]{1,0:T(8,128)(2,1)} %up.1, bf16[2048,128]{1,0:T(8,128)(2,1)} %down.1), custom_call_target="tpu_custom_call" | custom-call | flops 6442450944 | bytes 33554432 | tf_op jit(solution)/shard_map/pallas_call | solution.py:447
  118.1 0.0 copy-done
  118.1 0.0 copy-start.2
  118.1 2.2 %multiply_add_fusion = f32[128,2048]{1,0:T(8,128)} fusion(f32[128,2048]{1,0:T(8,128)S(1)} %copy-done, bf16[128,2048]{1,0:T(8,128)(2,1)} %get-tuple-element.8), kind=kLoop, calls=%fused_computation | loop fusion | flops 786432 | bytes 2621440 | tf_op jit(solution)/shard_map/add | solution.py:487
  120.3 0.0 copy-done.2
  120.3 0.0 copy-start.1
  120.3 0.8 copy.11
  121.1 0.4 copy-done.1
  121.5 0.8 copy.12
Async XLA Ops:
  0.6 117.4 %copy-start = (f32[128,2048]{1,0:T(8,128)S(1)}, f32[128,2048]{1,0:T(8,128)}, u32[]{:S(2)}) copy-start(f32[128,2048]{1,0:T(8,128)} %param.11) | copy-start | bytes 3145732
  118.1 2.2 %copy-start.2 = (bf16[128,2048]{1,0:T(8,128)(2,1)S(1)}, bf16[128,2048]{1,0:T(8,128)(2,1)}, u32[]{:S(2)}) copy-start(bf16[128,2048]{1,0:T(8,128)(2,1)} %get-tuple-element.12) | copy-start | bytes 1572868
  120.3 1.2 %copy-start.1 = (bf16[128,2048]{1,0:T(8,128)(2,1)S(1)}, bf16[128,2048]{1,0:T(8,128)(2,1)}, u32[]{:S(2)}) copy-start(bf16[128,2048]{1,0:T(8,128)(2,1)} %get-tuple-element.13) | copy-start | bytes 1572868
